TPU v7x, 32 devices: a whole 2x2x4 slice. The times are simulated.
32 devices in a mesh: ep: 4 (over y, x), tp: 8 (over z, core).
Axes of the slice: x: 2, y: 2, z: 4, core: 2. Of those that a mesh axis runs over, the one named last changes fastest.
Arguments:
- tokens: bfloat16 [1024, 2048], P('ep', 'tp'), may hold values from -600 to 600
- pre_gain: float32 [2048], P('tp'), may hold values from 0.1 to 1.9
- expert_gate: bfloat16 [4, 2048, 8192], P('ep', None, 'tp'), may hold values from -0.125 to 0.125
- expert_up: bfloat16 [4, 2048, 8192], P('ep', None, 'tp'), may hold values from -0.125 to 0.125
- expert_down: bfloat16 [4, 8192, 2048], P('ep', 'tp'), may hold values from -8 to 8
- routes: int32 [1024, 2], P('ep'), may hold values from 0 to 3, all different within a row; in each aligned block of 256 rows (0 to 255, 256 to 511, ...) at most 192 rows name the same one
- route_weights: float32 [1024, 2], P('ep'), may hold values from 0.1 to 1
- post_gain: float32 [2048], P('tp'), may hold values from 0.1 to 1.9
Outputs:
- layer_out: bfloat16 [1024, 2048], P('ep', 'tp')
Inputs may be any that keep to these rules, and one draw needn't show every extreme that they name: `routes`: each token names 2 different experts. Among the 256 tokens of one index of ep no expert is named more than 192 times, a bound that some expert reaches in some of these blocks.
All inputs are finite; a program needn't handle non-finite values.
Results may differ from a plain program's by a relative error of at most 0.024.
Values may be sent and summed in bfloat16 or wider, within the bound.
A program may use at most 64 MiB of HBM per device.

v0:
```python
import jax
import jax.numpy as jnp
from jax import lax
from jax.sharding import PartitionSpec as P

EPSILON = 1e-06


def local(tokens, pre_gain, expert_gate, expert_up, expert_down, routes, route_weights, post_gain):
    local_experts = expert_gate.shape[0]
    groups = lax.axis_size("ep")
    experts_all = local_experts * groups
    tok_rows, part_width = tokens.shape
    full_width = part_width * lax.axis_size("tp")
    capacity = 3 * tok_rows // experts_all
    values = tokens.astype(jnp.float32)
    input_sq = lax.psum(jnp.sum(values * values, axis=-1), "tp")
    normed = (
        values * lax.rsqrt(input_sq / full_width + EPSILON)[:, None] * pre_gain[None, :]
    ).astype(jnp.bfloat16)
    onehot = (routes[:, :, None] == jnp.arange(experts_all, dtype=jnp.int32)).astype(jnp.int32)
    onehot = onehot.reshape(tok_rows * 2, experts_all)
    earlier = jnp.cumsum(onehot, axis=0) - onehot
    slots = jnp.sum(earlier * onehot, axis=-1).reshape(tok_rows, 2)
    positions = routes * capacity + slots
    places = jnp.arange(experts_all * capacity, dtype=jnp.int32)
    first_pick = (places[:, None] == positions[None, :, 0]).astype(jnp.bfloat16)
    second_pick = (places[:, None] == positions[None, :, 1]).astype(jnp.bfloat16)
    dispatch = first_pick + second_pick
    outgoing = jnp.dot(dispatch, normed, preferred_element_type=jnp.float32).astype(jnp.bfloat16)
    arrived = lax.all_to_all(outgoing, "ep", split_axis=0, concat_axis=0, tiled=True)
    fragment = lax.all_gather(arrived, "tp", axis=1, tiled=True)
    count = fragment.shape[1]
    grouped = fragment.reshape(groups, local_experts, capacity, count)
    gate_pre = jnp.einsum(
        "secw,ewf->secf", grouped, expert_gate, preferred_element_type=jnp.float32
    )
    up_pre = jnp.einsum("secw,ewf->secf", grouped, expert_up, preferred_element_type=jnp.float32)
    hidden = (jax.nn.silu(gate_pre) * up_pre).astype(jnp.bfloat16)
    product = jnp.einsum("secf,efd->dsec", hidden, expert_down, preferred_element_type=jnp.float32)
    summed = lax.psum_scatter(
        product.reshape(lax.axis_size("tp") * part_width, groups * local_experts * capacity).astype(
            jnp.bfloat16
        ),
        "tp",
        scatter_dimension=0,
        tiled=True,
    )
    returned = lax.all_to_all(summed, "ep", split_axis=1, concat_axis=1, tiled=True)
    contract = (((0,), (1,)), ((), ()))
    first_out = lax.dot_general(first_pick, returned, contract, preferred_element_type=jnp.float32)
    second_out = lax.dot_general(
        second_pick, returned, contract, preferred_element_type=jnp.float32
    )
    combined = route_weights[:, 0:1] * first_out + route_weights[:, 1:2] * second_out
    output_sq = lax.psum(jnp.sum(combined * combined, axis=-1), "tp")
    scaled = combined * lax.rsqrt(output_sq / full_width + EPSILON)[:, None] * post_gain[None, :]
    return scaled.astype(jnp.bfloat16)


def solution(mesh):
    placed = (
        P("ep", "tp"),
        P("tp"),
        P("ep", None, "tp"),
        P("ep", None, "tp"),
        P("ep", "tp", None),
        P("ep", None),
        P("ep", None),
        P("tp"),
    )
    return jax.shard_map(
        local, mesh=mesh, in_specs=placed, out_specs=P("ep", "tp"), check_vma=False
    )
```

profile of v0, /device:TPU:0, one launch (start us, length us, event | category | flops | bytes accessed | tf_op | source)
XLA Modules:
  0.0 164.0 jit_solution(8557718616161930768)
XLA Ops:
  6.5 0.0 all-gather.2.cloned.1.call-start
  6.5 0.8 copy.20
  7.4 0.1 eq.61
  7.5 0.1 eq.57
  7.7 1.2 reduce-window.6
  8.9 0.2 slice_reduce_fusion
  9.1 0.2 reduce-window.9
  9.3 0.1 add_bitcast_fusion
  9.4 0.1 reshape.55
  9.5 0.1 copy.22
  9.6 0.7 multiply_add_fusion
  10.3 1.0 fusion.28
  11.3 18.1 %psum.14 = f32[256]{0:T(256)S(1)} all-reduce(f32[256]{0:T(256)S(1)} %fusion.28), channel_id=1, replica_groups=mesh['ep'=4,'tp'=8] {'tp'}, use_global_device_ids=true, to_apply=%region_4.5 | all-reduce | flops 256 | bytes 2048 | tf_op jit(solution)/shard_map/psum | solution.py:17
  29.4 1.3 convolution_convert_fusion
  30.7 10.1 %all_to_all.24 = bf16[4,192,256]{2,1,0:T(8,128)(2,1)} all-to-all(bf16[4,192,256]{2,1,0:T(8,128)(2,1)S(1)} %bitcast.82), channel_id=1, replica_groups=mesh['ep'=4,'tp'=8] {'ep'}, dimensions={0} | all-to-all | bytes 786432 | tf_op jit(solution)/shard_map/all_to_all | solution.py:31
  40.8 0.0 all-gather.2.cloned.1.call-update
  40.8 0.0 reduce-scatter.2.cloned.1.call-start
  40.8 35.9 %all-gather.2.cloned.1.call-done = bf16[768,2048]{1,0:T(8,128)(2,1)} async-done(((bf16[768,256]{1,0:T(8,128)(2,1)}), bf16[768,2048]{1,0:T(8,128)(2,1)}) %all-gather.2.cloned.1.call-update) | async-done | bytes 3145744 | tf_op jit(solution)/shard_map/all_gather | solution.py:32
  76.8 0.0 copy-start.2
  76.8 0.0 copy-start.4
  76.8 6.3 %fusion.2 = f32[4,192,1024]{2,1,0:T(8,128)S(1)} fusion(bf16[4,192,2048]{2,1,0:T(8,128)(2,1)} %bitcast.90, bf16[1,2048,1024]{2,1,0:T(8,128)(2,1)} %param.11), kind=kOutput, calls=%fused_computation.2 | convolution fusion | flops 3221225472 | bytes 10485760 | tf_op jit(solution)/shard_map/secw,ewf->secf/dot_general | solution.py:38
  83.1 0.0 copy-done.2
  83.1 0.0 copy-done.4
  83.1 0.0 copy-start.3
  83.1 3.8 %fusion.9 = bf16[4,1,192,1024]{3,2,0,1:T(8,128)(2,1)S(1)} fusion(f32[4,192,1024]{2,1,0:T(8,128)S(1)} %fusion.2, bf16[4,192,2048]{2,1,0:T(8,128)(2,1)S(1)} %bitcast.91, bf16[1,2048,1024]{2,1,0:T(8,128)(2,1)S(1)} %copy-done.2), kind=kOutput, calls=%fused_computation.8 | convolution fusion | flops 3225944064 | bytes 12058624 | tf_op jit(solution)/shard_map/secw,ewf->secf/dot_general | solution.py:35
  87.0 0.0 copy-done.3
  87.0 4.8 %fusion.13 = bf16[2048,768]{0,1:T(8,128)(2,1)} fusion(bf16[768,1024]{1,0:T(8,128)(2,1)S(1)} %bitcast.92, bf16[1,1024,2048]{2,1,0:T(8,128)(2,1)S(1)} %copy-done.3), kind=kOutput, calls=%fused_computation.14 | convolution fusion | flops 3222798336 | bytes 8912896 | tf_op jit(solution)/shard_map/secf,efd->dsec/dot_general | solution.py:40
  91.8 0.0 copy-start
  91.8 0.0 copy-start.1
  91.8 0.0 reduce-scatter.2.cloned.1.call-update
  91.8 38.8 %reduce-scatter.2.cloned.1.call-done = bf16[256,768]{0,1:T(8,128)(2,1)} async-done(((bf16[2048,768]{0,1:T(8,128)(2,1)}), bf16[256,768]{0,1:T(8,128)(2,1)}) %reduce-scatter.2.cloned.1.call-update) | async-done | bytes 393232 | tf_op jit(solution)/shard_map/reduce_scatter | solution.py:41
  130.6 3.6 %all-to-all-start.1 = ((bf16[256,4,192]{0,2,1:T(8,128)(2,1)}), bf16[256,4,192]{0,2,1:T(8,128)(2,1)S(1)}, u32[]{:S(2)}, u32[]{:S(2)}) async-start(bf16[256,4,192]{0,2,1:T(8,128)(2,1)} %bitcast.81), calls=%async_computation.2 | async-start | bytes 786432 | tf_op jit(solution)/shard_map/all_to_all | solution.py:49
  134.2 0.0 copy-done
  134.2 5.9 %all-to-all-done.1 = bf16[256,4,192]{0,2,1:T(8,128)(2,1)S(1)} async-done(((bf16[256,4,192]{0,2,1:T(8,128)(2,1)}), bf16[256,4,192]{0,2,1:T(8,128)(2,1)S(1)}, u32[]{:S(2)}, u32[]{:S(2)}) %all-to-all-start.1) | async-done | bytes 393248 | tf_op jit(solution)/shard_map/all_to_all | solution.py:49
  140.1 0.4 convolution_multiply_fusion.1
  140.5 0.4 multiply_reduce_fusion
  140.9 15.4 %psum.15 = f32[256]{0:T(256)S(1)} all-reduce(f32[256]{0:T(256)S(1)} %get-tuple-element.9), channel_id=1, replica_groups=mesh['ep'=4,'tp'=8] {'tp'}, use_global_device_ids=true, to_apply=%region_7.8 | all-reduce | flops 256 | bytes 2048 | tf_op jit(solution)/shard_map/psum | solution.py:56
  156.3 0.0 copy-done.1
  156.3 0.1 multiply_convert_fusion
  156.4 0.8 copy.23
  (6 shorter events, 0.1 us)
Async XLA Ops:
  6.5 70.3 %all-gather.2.cloned.1.call-start = ((), (), s32[]{:S(2)}) async-start(), calls=%async_computation.3 | async-start | bytes 3538944 | tf_op jit(solution)/shard_map/all_gather | solution.py:32
  40.8 89.8 %reduce-scatter.2.cloned.1.call-start = ((), (), s32[]{:S(2)}) async-start(), calls=%async_computation.4 | async-start | bytes 3538944 | tf_op jit(solution)/shard_map/reduce_scatter | solution.py:41
  76.8 6.3 %copy-start.2 = (bf16[1,2048,1024]{2,1,0:T(8,128)(2,1)S(1)}, bf16[1,2048,1024]{2,1,0:T(8,128)(2,1)}, u32[]{:S(2)}) copy-start(bf16[1,2048,1024]{2,1,0:T(8,128)(2,1)} %param.10) | copy-start | bytes 12582916
  76.8 6.3 %copy-start.4 = (bf16[768,2048]{1,0:T(8,128)(2,1)S(1)}, bf16[768,2048]{1,0:T(8,128)(2,1)}, u32[]{:S(2)}) copy-start(bf16[768,2048]{1,0:T(8,128)(2,1)} %all-gather.2.cloned.1.call-done) | copy-start | bytes 9437188
  83.1 3.9 %copy-start.3 = (bf16[1,1024,2048]{2,1,0:T(8,128)(2,1)S(1)}, bf16[1,1024,2048]{2,1,0:T(8,128)(2,1)}, u32[]{:S(2)}) copy-start(bf16[1,1024,2048]{2,1,0:T(8,128)(2,1)} %param.12) | copy-start | bytes 12582916
  91.8 42.4 %copy-start = (f32[256,2]{0,1:T(2,128)S(1)}, f32[256,2]{0,1:T(2,128)}, u32[]{:S(2)}) copy-start(f32[256,2]{0,1:T(2,128)} %param.14) | copy-start | bytes 6148
  91.8 64.5 %copy-start.1 = (f32[256]{0:T(256)S(1)}, f32[256]{0:T(256)}, u32[]{:S(2)}) copy-start(f32[256]{0:T(256)} %param.15) | copy-start | bytes 3076
  130.6 9.5 %all-to-all-start.1 = ((bf16[256,4,192]{0,2,1:T(8,128)(2,1)}), bf16[256,4,192]{0,2,1:T(8,128)(2,1)S(1)}, u32[]{:S(2)}, u32[]{:S(2)}) async-start(bf16[256,4,192]{0,2,1:T(8,128)(2,1)} %bitcast.81), calls=%async_computation.2 | async-start | bytes 786432 | tf_op jit(solution)/shard_map/all_to_all | solution.py:49
Sparse Core Ops, SparseCore 0:
  40.9 35.8 all-gather.1
  91.9 38.5 reduce-scatter.1
where the time goes:
time: 164 us
  waiting for transfers between devices  80.6 us (49%)
  blocking collectives  43.6 us (27%)
  matrix products  17 us (10%)
  between operations  13.5 us (8%)
  starting transfers between devices  3.69 us (2%)
  other arithmetic  3.35 us (2%)
  local copies, waits for them, and re-layouts  2.31 us (1%)
    reduce_scatter x1, waiting for transfers between devices, local(): lax.psum_scatter(product.reshape(lax.axis_size('tp') * part_width, groups...  38.8 us
    all_gather x1, waiting for transfers between devices, local(): fragment = lax.all_gather(arrived, 'tp', axis=1, tiled=True)  35.9 us
    psum x1, blocking collectives, local(): input_sq = lax.psum(jnp.sum(values * values, axis=-1), 'tp')  18.1 us
    psum x1, blocking collectives, local(): output_sq = lax.psum(jnp.sum(combined * combined, axis=-1), 'tp')  15.4 us
    all_to_all x1, blocking collectives, local(): lax.all_to_all(outgoing, 'ep', split_axis=0, concat_axis=0, tiled=True)  10.1 us
    dot_general x1, matrix products, local(): jnp.einsum('secw,ewf->secf', grouped, expert_up, preferred_element_type=j...  6.28 us
    all_to_all x1, waiting for transfers between devices, local(): lax.all_to_all(summed, 'ep', split_axis=1, concat_axis=1, tiled=True)  5.87 us
    dot_general x1, matrix products, local(): jnp.einsum('secf,efd->dsec', hidden, expert_down, preferred_element_type=...  4.83 us
  transfers between devices with their start and end apart: 3, of which 3 were waited for; matrix products, arithmetic and copies ran while one was open for 0% of the time, Pallas kernels for 0%

commit v1 on v0

--- a/solution.py
+++ b/solution.py
@@ -1,6 +1,10 @@
+import functools
+
 import jax
 import jax.numpy as jnp
 from jax import lax
+from jax.experimental import pallas as pl
+from jax.experimental.pallas import tpu as pltpu
 from jax.sharding import PartitionSpec as P
 
 EPSILON = 1e-06
@@ -58,6 +62,367 @@
     return scaled.astype(jnp.bfloat16)
 
 
+CORES = 2
+F32 = jnp.float32
+BF16 = jnp.bfloat16
+EXACT = lax.Precision.HIGHEST
+MESH = pl.DeviceIdType.MESH
+
+
+def flip(index, bits):
+    place = 1
+    while place <= bits:
+        if bits & place:
+            index = index + place - 2 * place * lax.rem(lax.div(index, place), 2)
+        place *= 2
+    return index
+
+
+def flip_traced(index, bits, size):
+    total, place = 0, 1
+    while place < size:
+        total = total + place * lax.rem(lax.div(index, place) + lax.div(bits, place), 2)
+        place *= 2
+    return total
+
+
+def fused(
+    groups, parts, tok, gain, route, weight, gate_hbm, up_hbm, down_hbm, post, out,
+    zbuf, gains, disp, mix, hi, lo, xsend, x, squares, gate, up, down, acc_gate, acc_up,
+    hidden, half, own, half_in, back, ret, zsend, zin, stats,
+    wsem, zs, zr, gs, gr, xs, xr, fs, fr, ds, dr, qs, qr, cs, cr, ps, pr,
+):
+    t, e = lax.axis_index("tp"), lax.axis_index("ep")
+    z, c = lax.div(t, CORES), lax.rem(t, CORES)
+    levels = parts // CORES
+    rows, width = tok.shape
+    cap = disp.shape[1]
+    full = parts * width
+
+    barrier = pltpu.get_barrier_semaphore()
+    for i in range(1, parts):
+        pl.semaphore_signal(barrier, inc=1, device_id={"tp": flip(t, i)}, device_id_type=MESH)
+    for d in range(1, groups):
+        pl.semaphore_signal(barrier, inc=1, device_id={"ep": flip(e, d)}, device_id_type=MESH)
+
+    loads = [
+        pltpu.make_async_copy(gate_hbm.at[0], gate, wsem.at[0]),
+        pltpu.make_async_copy(up_hbm.at[0], up, wsem.at[1]),
+        pltpu.make_async_copy(down_hbm.at[0], down, wsem.at[2]),
+    ]
+    for load in loads:
+        load.start()
+
+    def remote(src, dst, send, recv, **device):
+        return pltpu.make_async_remote_copy(
+            src_ref=src, dst_ref=dst, send_sem=send, recv_sem=recv,
+            device_id=device, device_id_type=MESH,
+        )
+
+    def token_copy(j, level):
+        return remote(tok, zbuf.at[level], zs.at[j], zr.at[level], tp=flip(z, j) * CORES + c)
+
+    def gain_copy(i, part):
+        return remote(gain, gains.at[part], gs.at[i], gr.at[part], tp=flip(t, i))
+
+    def row_copy(j, d, source):
+        level = flip(z, j)
+        return remote(
+            xsend.at[j, d], x.at[level * CORES + c, source],
+            xs.at[j, d], xr.at[level, source], ep=flip(e, d),
+        )
+
+    def core_copy(level, source, core):
+        slot = x.at[level * CORES + core, source]
+        return remote(slot, slot, fs.at[level, source], fr.at[level, source], tp=z * CORES + 1 - c)
+
+    def half_copy(source):
+        return remote(
+            half.at[source], half_in.at[source], ds.at[source], dr.at[source],
+            tp=z * CORES + 1 - c,
+        )
+
+    def back_copy(level, source, expert):
+        return remote(
+            back.at[source, level], ret.at[level, expert],
+            qs.at[source, level], qr.at[level, expert], ep=source,
+        )
+
+    def sum_copy(j, level):
+        return remote(zsend.at[j], zin.at[level], cs.at[j], cr.at[level], tp=flip(z, j) * CORES + c)
+
+    def stat_copy(i, part):
+        return remote(stats.at[t], stats.at[part], ps.at[i], pr.at[part], tp=flip(t, i))
+
+    zbuf[z] = tok[...]
+    gains[t] = gain[...]
+    r = route[...]
+    first, second = r[0:1], r[1:2]
+    w = weight[...]
+    names = lax.broadcasted_iota(jnp.int32, (8, rows), 0)
+    member = jnp.where((names == first) | (names == second), 1.0, 0.0)
+    before = jnp.where(
+        lax.broadcasted_iota(jnp.int32, (rows, rows), 0)
+        < lax.broadcasted_iota(jnp.int32, (rows, rows), 1),
+        1.0, 0.0,
+    )
+    slots = jnp.dot(member.astype(BF16), before.astype(BF16), preferred_element_type=F32)
+    slots = jnp.where(member > 0.5, slots, -1.0).astype(jnp.int32)
+    lines = lax.broadcasted_iota(jnp.int32, (cap, rows), 0)
+    for k in range(groups):
+        disp[k] = jnp.where(lines == slots[k : k + 1], 1.0, 0.0).astype(BF16)
+
+    pl.semaphore_wait(barrier, parts + groups - 2)
+    for j in range(1, levels):
+        token_copy(j, z).start()
+
+    def send(j):
+        level = flip(z, j)
+        if j > 0:
+            token_copy(j, level).wait_recv()
+        block = zbuf[level]
+        for d in range(groups - 1, -1, -1):
+            picked = jnp.dot(disp[flip(e, d)], block, preferred_element_type=F32).astype(BF16)
+            if d:
+                xsend[j, d] = picked
+                row_copy(j, d, e).start()
+            else:
+                x[level * CORES + c, e] = picked
+                core_copy(level, e, c).start()
+
+    def pass_on(j):
+        level = flip(z, j)
+        for d in range(groups - 1, 0, -1):
+            source = flip(e, d)
+            row_copy(j, d, source).wait_recv()
+            core_copy(level, source, c).start()
+
+    def project(j, source):
+        level = flip(z, j)
+        core_copy(level, source, 1 - c).wait_recv()
+        total, gate_part, up_part = None, None, None
+        for core in range(CORES):
+            part = level * CORES + core
+            values = x[part, source].astype(F32)
+            square = values * values
+            for lane in range(0, width, 128):
+                piece = square[:, lane : lane + 128]
+                total = piece if total is None else total + piece
+            scaled = (values * gains[part]).astype(BF16)
+            depth = pl.ds(pl.multiple_of(part * width, 128), width)
+            gate_new = jnp.dot(scaled, gate[depth, :], preferred_element_type=F32)
+            up_new = jnp.dot(scaled, up[depth, :], preferred_element_type=F32)
+            gate_part = gate_new if gate_part is None else gate_part + gate_new
+            up_part = up_new if up_part is None else up_part + up_new
+        if j > 0:
+            total = total + squares[source]
+            gate_part = gate_part + acc_gate[source]
+            up_part = up_part + acc_up[source]
+        return total, gate_part, up_part
+
+    def collect(j):
+        def body(i, carry):
+            source = flip_traced(e, groups - 1 - i, groups)
+            squares[source], acc_gate[source], acc_up[source] = project(j, source)
+            return carry
+
+        pass_on(j)
+        lax.fori_loop(0, groups, body, 0)
+
+    send(0)
+    for i in range(1, parts):
+        gain_copy(i, t).start()
+    for k in range(groups):
+        chosen = jnp.where(first == k, w[0:1], w[1:2])
+        mix[k * cap : (k + 1) * cap, :] = jnp.where(lines == slots[k : k + 1], chosen, 0.0)
+    turned = mix[...].T
+    high = turned.astype(BF16)
+    hi[...] = high
+    lo[...] = (turned - high.astype(F32)).astype(BF16)
+    for j in range(1, levels):
+        send(j)
+        if j == 1:
+            for i in range(1, parts):
+                gain_copy(i, flip(t, i)).wait_recv()
+            loads[0].wait()
+            loads[1].wait()
+        collect(j - 1)
+
+    def reduce(source):
+        half_copy(source).wait_recv()
+        for j in range(levels - 1, -1, -1):
+            level = flip(z, j)
+            summed = (own[source, level] + half_in[source, level].astype(F32)).astype(BF16)
+            yield j, level, summed
+
+    def expert(i, carry):
+        source = flip_traced(e, groups - 1 - i, groups)
+        total, gate_part, up_part = project(levels - 1, source)
+        scale = lax.rsqrt(jnp.sum(total, axis=1, keepdims=True) / full + EPSILON)
+        gate_part = gate_part * scale
+        hidden[...] = (
+            gate_part / (1.0 + jnp.exp(-gate_part)) * (up_part * scale)
+        ).astype(BF16)
+
+        def down_block(level, core):
+            columns = pl.ds(pl.multiple_of((level * CORES + core) * width, 128), width)
+            return jnp.dot(hidden[...], down[:, columns], preferred_element_type=F32)
+
+        for level in range(levels):
+            half[source, level] = down_block(level, 1 - c).astype(BF16)
+        half_copy(source).start()
+        for level in range(levels):
+            own[source, level] = down_block(level, c)
+
+        @pl.when(i > 0)
+        def _():
+            earlier = flip_traced(e, groups - i, groups)
+            for _, level, summed in reduce(earlier):
+                back[earlier, level] = summed
+                back_copy(level, earlier, e).start()
+
+        return carry
+
+    pass_on(levels - 1)
+    loads[2].wait()
+    lax.fori_loop(0, groups, expert, 0)
+    for _, level, summed in reduce(e):
+        ret[level, e] = summed
+
+    combined = None
+    for j in range(levels - 1, -1, -1):
+        level = flip(z, j)
+        for d in range(groups - 1, 0, -1):
+            source = flip(e, d)
+            back_copy(level, source, source).wait_recv()
+        results = ret[level].reshape(groups * cap, width)
+        combined = jnp.dot(hi[...], results, preferred_element_type=F32) + jnp.dot(
+            lo[...], results, preferred_element_type=F32
+        )
+        if j:
+            zsend[j] = combined.astype(BF16)
+            sum_copy(j, z).start()
+    for j in range(levels - 1, 0, -1):
+        level = flip(z, j)
+        sum_copy(j, level).wait_recv()
+        combined = combined + zin[level].astype(F32)
+    stats[t] = lax.dot_general(
+        jnp.ones((8, width), F32), combined * combined, (((1,), (1,)), ((), ())),
+        precision=EXACT, preferred_element_type=F32,
+    )
+    for i in range(1, parts):
+        stat_copy(i, t).start()
+    for i in range(1, parts):
+        stat_copy(i, flip(t, i)).wait_recv()
+    total = jnp.sum(stats[...], axis=0)
+    column = lax.dot_general(
+        total, jnp.full((8, 128), 0.125, F32), (((0,), (0,)), ((), ())),
+        precision=EXACT, preferred_element_type=F32,
+    )
+    scale = lax.rsqrt(column[:, 0:1] / full + EPSILON)
+    out[...] = (combined * scale * post[...]).astype(BF16)
+
+    for j in range(1, levels):
+        token_copy(j, z).wait_send()
+        sum_copy(j, z).wait_send()
+    for i in range(1, parts):
+        gain_copy(i, t).wait_send()
+        stat_copy(i, t).wait_send()
+    for j in range(levels):
+        for d in range(1, groups):
+            row_copy(j, d, e).wait_send()
+            back_copy(j, flip(e, d), e).wait_send()
+        for k in range(groups):
+            core_copy(j, k, c).wait_send()
+    for k in range(groups):
+        half_copy(k).wait_send()
+
+
+def local_fused(tokens, pre_gain, expert_gate, expert_up, expert_down, routes, route_weights, post_gain):
+    groups, parts = lax.axis_size("ep"), lax.axis_size("tp")
+    rows, width = tokens.shape
+    _, features, units = expert_gate.shape
+    levels = parts // CORES
+    cap = 3 * rows // groups
+    vmem = pl.BlockSpec(memory_space=pltpu.VMEM)
+    anywhere = pl.BlockSpec(memory_space=pl.ANY)
+    dma = pltpu.SemaphoreType.DMA
+    block = (levels, groups, cap, width)
+    by_source = (groups, levels, cap, width)
+    return pl.pallas_call(
+        functools.partial(fused, groups, parts),
+        out_shape=jax.ShapeDtypeStruct((rows, width), BF16),
+        in_specs=[vmem] * 4 + [anywhere] * 3 + [vmem],
+        out_specs=vmem,
+        scratch_shapes=[
+            pltpu.VMEM((levels, rows, width), BF16),
+            pltpu.VMEM((parts, 1, width), F32),
+            pltpu.VMEM((groups, cap, rows), BF16),
+            pltpu.VMEM((groups * cap, rows), F32),
+            pltpu.VMEM((rows, groups * cap), BF16),
+            pltpu.VMEM((rows, groups * cap), BF16),
+            pltpu.VMEM(block, BF16),
+            pltpu.VMEM((parts, groups, cap, width), BF16),
+            pltpu.VMEM((groups, cap, 128), F32),
+            pltpu.VMEM((features, units), BF16),
+            pltpu.VMEM((features, units), BF16),
+            pltpu.VMEM((units, features), BF16),
+            pltpu.VMEM((groups, cap, units), F32),
+            pltpu.VMEM((groups, cap, units), F32),
+            pltpu.VMEM((cap, units), BF16),
+            pltpu.VMEM(by_source, BF16),
+            pltpu.VMEM(by_source, F32),
+            pltpu.VMEM(by_source, BF16),
+            pltpu.VMEM(by_source, BF16),
+            pltpu.VMEM(block, BF16),
+            pltpu.VMEM((levels, rows, width), BF16),
+            pltpu.VMEM((levels, rows, width), BF16),
+            pltpu.VMEM((parts, 8, rows), F32),
+            dma((3,)),
+            dma((levels,)), dma((levels,)),
+            dma((parts,)), dma((parts,)),
+            dma((levels, groups)), dma((levels, groups)),
+            dma((levels, groups)), dma((levels, groups)),
+            dma((groups,)), dma((groups,)),
+            dma((groups, levels)), dma((levels, groups)),
+            dma((levels,)), dma((levels,)),
+            dma((parts,)), dma((parts,)),
+        ],
+        compiler_params=pltpu.CompilerParams(
+            collective_id=0, has_side_effects=True, vmem_limit_bytes=60 * 1024 * 1024
+        ),
+    )(
+        tokens, pre_gain.reshape(1, width), routes.T, route_weights.T,
+        expert_gate, expert_up, expert_down, post_gain.reshape(1, width),
+    )
+
+
+def power_of_two(count):
+    return count & (count - 1) == 0
+
+
+def plan(mesh):
+    def choose(*args):
+        tokens, gate = args[0], args[2]
+        groups, parts = mesh.shape["ep"], mesh.shape["tp"]
+        rows, width = tokens.shape
+        fits = (
+            gate.shape[0] == 1
+            and power_of_two(groups)
+            and power_of_two(parts)
+            and 2 <= groups <= 8
+            and parts >= 2 * CORES
+            and width % 128 == 0
+            and rows % 128 == 0
+            and (3 * rows // groups) % 16 == 0
+            and (3 * rows) % 128 == 0
+            and gate.shape[2] % 128 == 0
+        )
+        return (local_fused if fits else local)(*args)
+
+    return choose
+
+
 def solution(mesh):
     placed = (
         P("ep", "tp"),
@@ -70,5 +435,5 @@
         P("tp"),
     )
     return jax.shard_map(
-        local, mesh=mesh, in_specs=placed, out_specs=P("ep", "tp"), check_vma=False
-    )
+        plan(mesh), mesh=mesh, in_specs=placed, out_specs=P("ep", "tp"), check_vma=False
+    )

time: 164 us -> 73.2 us (0.45)
  waiting for transfers between devices: 80.6 us -> 0 us
  Pallas kernels: 0 us -> 71.5 us
  blocking collectives: 43.6 us -> 0 us
  matrix products: 17 us -> 0 us
  between operations: 13.5 us -> 0.01 us
  starting transfers between devices: 3.69 us -> 0 us
  other arithmetic: 3.35 us -> 0 us
    pallas_call x0 -> x1, Pallas kernels: none -> 71.5 us  [local_fused(): pl.pallas_call(functools.partial(fused, groups, parts), out_shape=jax.Sha...]
    reduce_scatter x1 -> x0, waiting for transfers between devices: 38.8 us -> none  [local(): lax.psum_scatter(product.reshape(lax.axis_size('tp') * part_width, groups...]
    all_gather x1 -> x0, waiting for transfers between devices: 35.9 us -> none  [local(): fragment = lax.all_gather(arrived, 'tp', axis=1, tiled=True)]
    psum x2 -> x0, blocking collectives: 33.6 us -> none  [the longest x1 18.1 us: local(): input_sq = lax.psum(jnp.sum(values * values, axis=-1), 'tp')]
    dot_general x6 -> x0, matrix products: 17 us -> none  [the longest x1 6.28 us: local(): jnp.einsum('secw,ewf->secf', grouped, expert_up, preferred_element_type=j...]
    all_to_all x1 -> x0, blocking collectives: 10.1 us -> none  [local(): lax.all_to_all(outgoing, 'ep', split_axis=0, concat_axis=0, tiled=True)]
    all_to_all x1 -> x0, waiting for transfers between devices: 5.87 us -> none  [local(): lax.all_to_all(summed, 'ep', split_axis=1, concat_axis=1, tiled=True)]
    all_to_all x1 -> x0, starting transfers between devices: 3.64 us -> none  [local(): lax.all_to_all(summed, 'ep', split_axis=1, concat_axis=1, tiled=True)]
  transfers between devices with their start and end apart: 3 -> 0, of which waited for: 3 -> 0; matrix products, arithmetic and copies ran while one was open for 0% -> 0% of each run, Pallas kernels for 0% -> 0%
where the time goes in v1:
time: 73.2 us; the launch traced here: 73.1 us
  Pallas kernels  71.5 us (98%)
  local copies, waits for them, and re-layouts  1.57 us (2%)
    pallas_call x1, Pallas kernels, local_fused(): pl.pallas_call(functools.partial(fused, groups, parts), out_shape=jax.Sha...  71.5 us
    unnamed x1, local copies, waits for them, and re-layouts  1.57 us

profile of v1, /device:TPU:0, one launch (start us, length us, event | category | flops | bytes accessed | tf_op | source)
XLA Modules:
  0.0 73.1 jit_solution(9939850911873049757)
XLA Ops:
  0.0 71.5 %shard_map.82 = bf16[256,256]{1,0:T(8,128)(2,1)} custom-call(bf16[256,256]{1,0:T(8,128)(2,1)} %tok.1, f32[1,256]{1,0:T(1,128)} %bitcast.6, s32[2,256]{1,0:T(2,128)} %bitcast.4, f32[2,256]{1,0:T(2,128)} %bitcast.5, bf16[1,2048,1024]{2,1,0:T(8,128)(2,1)} %gate_hbm.1, bf16[1,2048,1024]{2,1,0:T(8,128)(2,1)} %up_hbm.1, bf16[1,1024,2048]{2,1,0:T(8,128)(2,1)} %down_hbm.1, ...), custom_call_target="tpu_custom_call" | custom-call | tf_op jit(solution)/shard_map/pallas_call | solution.py:352
  71.5 1.6 %copy.10 = bf16[256,256]{1,0:T(8,128)(2,1)} copy(bf16[256,256]{1,0:T(8,128)(2,1)} %shard_map.82) | data formatting | bytes 262144

commit v2 on v1

--- a/solution.py
+++ b/solution.py
@@ -119,8 +119,29 @@
             device_id=device, device_id_type=MESH,
         )
 
-    def token_copy(j, level):
-        return remote(tok, zbuf.at[level], zs.at[j], zr.at[level], tp=flip(z, j) * CORES + c)
+    def token_copy(level, up):
+        step = 1 if up else -1
+        source = zbuf.at[level]
+        return remote(source, source, zs.at[level, int(up)], zr.at[level], tp=t + step * CORES)
+
+    def relay(k):
+        @pl.when(z >= k)
+        def _():
+            if k:
+                token_copy(z - k, True).wait_recv()
+
+            @pl.when(z < levels - 1)
+            def _():
+                token_copy(z - k, True).start()
+
+        @pl.when(z + k < levels)
+        def _():
+            if k:
+                token_copy(z + k, False).wait_recv()
+
+            @pl.when(z > 0)
+            def _():
+                token_copy(z + k, False).start()
 
     def gain_copy(i, part):
         return remote(gain, gains.at[part], gs.at[i], gr.at[part], tp=flip(t, i))
@@ -173,13 +194,12 @@
         disp[k] = jnp.where(lines == slots[k : k + 1], 1.0, 0.0).astype(BF16)
 
     pl.semaphore_wait(barrier, parts + groups - 2)
-    for j in range(1, levels):
-        token_copy(j, z).start()
+    relay(0)
 
     def send(j):
         level = flip(z, j)
         if j > 0:
-            token_copy(j, level).wait_recv()
+            relay(j)
         block = zbuf[level]
         for d in range(groups - 1, -1, -1):
             picked = jnp.dot(disp[flip(e, d)], block, preferred_element_type=F32).astype(BF16)
@@ -322,8 +342,17 @@
     scale = lax.rsqrt(column[:, 0:1] / full + EPSILON)
     out[...] = (combined * scale * post[...]).astype(BF16)
 
+    for j in range(levels):
+
+        @pl.when((z >= j) & (z < levels - 1))
+        def _():
+            token_copy(j, True).wait_send()
+
+        @pl.when((z <= j) & (z > 0))
+        def _():
+            token_copy(j, False).wait_send()
+
     for j in range(1, levels):
-        token_copy(j, z).wait_send()
         sum_copy(j, z).wait_send()
     for i in range(1, parts):
         gain_copy(i, t).wait_send()
@@ -379,7 +408,7 @@
             pltpu.VMEM((levels, rows, width), BF16),
             pltpu.VMEM((parts, 8, rows), F32),
             dma((3,)),
-            dma((levels,)), dma((levels,)),
+            dma((levels, 2)), dma((levels,)),
             dma((parts,)), dma((parts,)),
             dma((levels, groups)), dma((levels, groups)),
             dma((levels, groups)), dma((levels, groups)),

time: 73.2 us -> 67.1 us (0.917)
  Pallas kernels: 71.5 us -> 65.4 us
    pallas_call x1, Pallas kernels: 71.5 us -> 65.4 us  [local_fused(): pl.pallas_call(functools.partial(fused, groups, parts), out_shape=jax.Sha...]
where the time goes in v2:
time: 67.1 us; the launch traced here: 67 us
  Pallas kernels  65.4 us (97%)
  local copies, waits for them, and re-layouts  1.57 us (2%)
    pallas_call x1, Pallas kernels, local_fused(): pl.pallas_call(functools.partial(fused, groups, parts), out_shape=jax.Sha...  65.4 us
    unnamed x1, local copies, waits for them, and re-layouts  1.57 us

profile of v2, /device:TPU:0, one launch (start us, length us, event | category | flops | bytes accessed | tf_op | source)
XLA Modules:
  0.0 67.0 jit_solution(1132376372315102964)
XLA Ops:
  0.0 65.4 %shard_map.82 = bf16[256,256]{1,0:T(8,128)(2,1)} custom-call(bf16[256,256]{1,0:T(8,128)(2,1)} %tok.1, f32[1,256]{1,0:T(1,128)} %bitcast.6, s32[2,256]{1,0:T(2,128)} %bitcast.4, f32[2,256]{1,0:T(2,128)} %bitcast.5, bf16[1,2048,1024]{2,1,0:T(8,128)(2,1)} %gate_hbm.1, bf16[1,2048,1024]{2,1,0:T(8,128)(2,1)} %up_hbm.1, bf16[1,1024,2048]{2,1,0:T(8,128)(2,1)} %down_hbm.1, ...), custom_call_target="tpu_custom_call" | custom-call | tf_op jit(solution)/shard_map/pallas_call | solution.py:381
  65.4 1.6 %copy.10 = bf16[256,256]{1,0:T(8,128)(2,1)} copy(bf16[256,256]{1,0:T(8,128)(2,1)} %shard_map.82) | data formatting | bytes 262144
